TPU v7x, 32 devices: a whole 2x2x4 slice. The times are simulated.
32 devices in a mesh: fs: 8 (over z, y), tp: 4 (over x, core).
Axes of the slice: x: 2, y: 2, z: 4, core: 2. Of those that a mesh axis runs over, the one named last changes fastest.
Arguments:
- tokens: bfloat16 [1280, 2048], P('fs', 'tp'), may hold values from -6 to 6
- mix_gain: float32 [2048], replicated, may hold values from 0.1 to 1.9
- in_x_w: bfloat16 [2048, 1024], P('fs', 'tp'), may hold values from -0.125 to 0.125
- in_gate_w: bfloat16 [2048, 1024], P('fs', 'tp'), may hold values from -0.125 to 0.125
- conv_taps: float32 [4, 1024], P(None, 'tp'), may hold values from -3 to 3
- gate_x_blocks: bfloat16 [8, 128, 128], P('tp'), may hold values from -0.5 to 0.5
- gate_a_blocks: bfloat16 [8, 128, 128], P('tp'), may hold values from -0.5 to 0.5
- forget_rate: float32 [1024], P('tp'), may hold values from 0.002 to 0.08
- out_w: bfloat16 [1024, 2048], P('tp', 'fs'), may hold values from -0.1875 to 0.1875
- ffn_gain: float32 [2048], replicated, may hold values from 0.1 to 1.9
- ffn_gate_w: bfloat16 [2048, 2816], P('fs', 'tp'), may hold values from -0.125 to 0.125
- ffn_up_w: bfloat16 [2048, 2816], P('fs', 'tp'), may hold values from -0.125 to 0.125
- ffn_down_w: bfloat16 [2816, 2048], P('tp', 'fs'), may hold values from -0.109375 to 0.109375
Outputs:
- layer_out: bfloat16 [1280, 2048], P('fs', 'tp')
All inputs are finite; a program needn't handle non-finite values.
Results may differ from a plain program's by a relative error of at most 0.015.
Values may be sent and summed in bfloat16 or wider, within the bound.
A program may use at most 64 MiB of HBM per device.

v0:
```python
import functools

import jax
import jax.numpy as jnp
from jax import lax
from jax.experimental import pallas as pl
from jax.experimental.pallas import tpu as pltpu
from jax.sharding import PartitionSpec as P

LANES = 128

epsilon = 1e-06
gate_power = 8.0


def rms_norm(values, gain):
    wide = values.astype(jnp.float32)
    mean_square = jnp.mean(wide * wide, axis=-1, keepdims=True)
    return (wide * lax.rsqrt(mean_square + epsilon) * gain).astype(jnp.bfloat16)


def full_rows(shard):
    return lax.all_gather(shard, "tp", axis=1, tiled=True)


def pair_folder(left_rows, pieces):
    return (
        jnp.dot(left_rows, pieces[0], preferred_element_type=jnp.float32),
        jnp.dot(left_rows, pieces[1], preferred_element_type=jnp.float32),
    )


def project_out(acts, weight):
    partial_terms = jnp.dot(
        acts, lax.all_gather(weight, "fs", axis=1, tiled=True), preferred_element_type=jnp.float32
    )
    return lax.psum_scatter(
        partial_terms.astype(jnp.bfloat16), "tp", scatter_dimension=1, tiled=True
    ).astype(jnp.float32)


def combine(earlier, later):
    return (earlier[0] * later[0], later[0] * earlier[1] + later[1])


def on_device(
    tokens,
    mix_gain,
    in_x_w,
    in_gate_w,
    conv_taps,
    gate_x_blocks,
    gate_a_blocks,
    forget_rate,
    out_w,
    ffn_gain,
    ffn_gate_w,
    ffn_up_w,
    ffn_down_w,
):
    normed = rms_norm(full_rows(tokens), mix_gain)
    length = normed.shape[0]
    chan_width = in_x_w.shape[1]
    branch_in, branch_gate = pair_folder(
        normed,
        (
            lax.all_gather(in_x_w, "fs", axis=0, tiled=True),
            lax.all_gather(in_gate_w, "fs", axis=0, tiled=True),
        ),
    )
    tap_count = conv_taps.shape[0]
    padded = jnp.pad(branch_in, ((tap_count - 1, 0), (0, 0)))
    conv_sum = padded[0:length] * conv_taps[0]
    for index in range(1, tap_count):
        conv_sum = conv_sum + padded[index : index + length] * conv_taps[index]
    conv_out = conv_sum.astype(jnp.bfloat16)
    blocks = gate_x_blocks.shape[0]
    block_dim = gate_x_blocks.shape[1]
    grouped = conv_out.reshape(length, blocks, block_dim)
    gate_x = jax.nn.sigmoid(
        jnp.einsum(
            "tbi,bij->tbj", grouped, gate_x_blocks, preferred_element_type=jnp.float32
        ).reshape(length, chan_width)
    )
    gate_a = jax.nn.sigmoid(
        jnp.einsum(
            "tbi,bij->tbj", grouped, gate_a_blocks, preferred_element_type=jnp.float32
        ).reshape(length, chan_width)
    )
    log_decay = -gate_power * gate_a * forget_rate
    decay = jnp.exp(log_decay)
    scale = jnp.sqrt(-jnp.expm1(2.0 * log_decay))
    scale = jnp.where((jnp.arange(length) == 0)[:, None], 1.0, scale)
    driven = conv_out.astype(jnp.float32) * gate_x * scale
    _, state = lax.associative_scan(combine, (decay, driven), axis=0)
    mixer_out = (state * jax.nn.gelu(branch_gate)).astype(jnp.bfloat16)
    after_mix = (tokens.astype(jnp.float32) + project_out(mixer_out, out_w)).astype(jnp.bfloat16)
    normed_ffn = rms_norm(full_rows(after_mix), ffn_gain)
    gate_val, up_val = pair_folder(
        normed_ffn,
        (
            lax.all_gather(ffn_gate_w, "fs", axis=0, tiled=True),
            lax.all_gather(ffn_up_w, "fs", axis=0, tiled=True),
        ),
    )
    hidden = (jax.nn.silu(gate_val) * up_val).astype(jnp.bfloat16)
    return (after_mix.astype(jnp.float32) + project_out(hidden, ffn_down_w)).astype(jnp.bfloat16)


def paired(mesh, tokens, mix_gain, in_x_w, in_gate_w, conv_taps, gate_x_blocks, *rest):
    ffn_down_w = rest[-1]
    return (
        mesh.shape["fs"] == 8
        and mesh.shape["tp"] == 4
        and gate_x_blocks.shape == (2, LANES, LANES)
        and tokens.shape[0] % 16 == 0
        and tokens.shape[1] % (2 * LANES) == 0
        and ffn_down_w.shape[0] % 32 == 0
    )


def kernel(
    tok, gain1, w_x, w_g, taps, gxb, gab, forget, w_out, gain2, w_gate, w_up, w_dn,
    result,
    x1, nb, win, wout, wgate, wup, wdn, s1, s1r, k1, x1r, zs1, z1r, after, mix, x2, hid,
    s2, s2r, k2, x2r, zs2, z2r,
    send_z, recv_z, send_y, recv_y, own_sem, ag_send, ag_recv, rs_send, rs_recv,
):
    f, t = lax.axis_index("fs"), lax.axis_index("tp")
    z, y = f // 2, f % 2
    h = z % 2
    rows, feats = tok.shape
    zs = (z, z + 1 - 2 * h, (z + 2) % 4, 3 - z)
    fz = tuple(zz * 2 + y for zz in zs)
    fy = z * 2 + 1 - y
    t_core = t + 1 - 2 * (t % 2)
    t_x = (t + 2) % 4
    t_xc = (t_core + 2) % 4
    model = x1.shape[1]

    barrier = pltpu.get_barrier_semaphore()
    peers = [(fz[1], t), (fz[2], t), (fz[3], t), (fy, t), (f, t_core), (f, t_x)]
    for peer in peers:
        pl.semaphore_signal(barrier, inc=1, device_id=peer, device_id_type=pl.DeviceIdType.MESH)
    pl.semaphore_wait(barrier, len(peers))

    started = []

    def send(src, dst, s_sem, r_sem, peer):
        copy = pltpu.make_async_remote_copy(
            src_ref=src, dst_ref=dst, send_sem=s_sem, recv_sem=r_sem,
            device_id=peer, device_id_type=pl.DeviceIdType.MESH,
        )
        copy.start()
        started.append(copy)
        return copy

    def span(index, width):
        return pl.ds(pl.multiple_of(index * width, width), width)

    depth = w_x.shape[0]
    cols = w_out.shape[1]
    half_ff = w_dn.shape[0] // 2
    fill = wdn.shape[0] - half_ff

    def piece(group, half):
        if group < 2:
            return (w_x, w_g)[group].at[:, span(half, LANES)]
        if group == 2:
            return w_out.at[span(half, LANES), :]
        return (w_gate, w_up, w_dn)[group - 3].at[span(half, half_ff), :]

    def place(group, source):
        if group < 2:
            return win.at[span(source, depth), pl.ds(group * LANES, LANES)]
        if group == 2:
            return wout.at[:, span(source, cols)]
        return (wgate, wup, wdn)[group - 3].at[pl.ds(0, half_ff), span(source, cols)]

    own_copies = {}
    z_copies = {}
    y_copies = {}

    def launch(group):
        for d in (1, 2, 3):
            half = h if d == 2 else 1 - h
            z_copies[group, d] = send(
                piece(group, half), place(group, f), send_z.at[group, d - 1], recv_z.at[group, d - 1], (fz[d], t)
            )
            if d == 1:
                y_copies[group, 0] = send(
                    piece(group, h), place(group, f), send_y.at[group, 0], recv_y.at[group, 0], (fy, t)
                )
        own_copies[group] = pltpu.make_async_copy(piece(group, h), place(group, f), own_sem.at[group])
        own_copies[group].start()

    def forward(group, d):
        z_copies[group, d].wait_recv()
        y_copies[group, d] = send(
            place(group, fz[d]), place(group, fz[d]), send_y.at[group, d], recv_y.at[group, d], (fy, t)
        )

    def arrive(group):
        own_copies[group].wait()
        for d in range(4):
            y_copies[group, d].wait_recv()

    cut = feats // 2
    mine, theirs = span(h, rows), span(1 - h, rows)

    def gather_start(k, own, x):
        def go(i, r, c, peer):
            src = own if i < 3 else x.at[r, span(c, feats)]
            return send(src, x.at[r, span(c, feats)], ag_send.at[k, i], ag_recv.at[k, i], peer)

        x_peer, core_peer = (f, t_x), (f, t_core)
        first = go(0, mine, t, (fz[1], t)), go(1, mine, t, x_peer), go(2, mine, t, core_peer)
        x[mine, span(t, feats)] = own[...]
        return go, first, x_peer, core_peer

    def gather_rest(state, hooks):
        go, (by_z, by_x, by_core), x_peer, core_peer = state
        by_z.wait_recv()
        c3 = go(3, theirs, t, x_peer)
        c4 = go(4, theirs, t, core_peer)
        hooks[0]()
        by_x.wait_recv()
        c5 = go(5, mine, t_x, core_peer)
        hooks[1]()
        c3.wait_recv()
        c6 = go(6, theirs, t_x, core_peer)
        hooks[2]()
        for c in (by_core, c4, c5, c6):
            c.wait_recv()

    def norm(x, gain, out):
        step = 32

        def one(i, carry):
            at = pl.ds(pl.multiple_of(i * step, step), step)
            wide = x[at, :].astype(jnp.float32)
            scale = lax.rsqrt(jnp.mean(wide * wide, axis=-1, keepdims=True) + epsilon)
            out[at, :] = (wide * scale * gain[...]).astype(jnp.bfloat16)
            return carry

        lax.fori_loop(0, x.shape[0] // step, one, 0)

    def scatter(k, acts, weight, s, r1, keep, r2, s3, r3, base, out, hooks):
        core_peer, x_peer = (f, t_core), (f, t_x)

        def project(block):
            at = span(block, feats)
            s[:, at] = jnp.dot(acts[...], weight[:, at], preferred_element_type=jnp.float32).astype(jnp.bfloat16)
            return s.at[:, at]

        a = send(project(t_xc), r1.at[0], rs_send.at[k, 0], rs_recv.at[k, 0], core_peer)
        b = send(project(t_core), r1.at[1], rs_send.at[k, 1], rs_recv.at[k, 1], core_peer)
        project(t_x)
        project(t)
        hooks[0]()
        a.wait_recv()
        keep[0] = (s[:, span(t_x, feats)].astype(jnp.float32) + r1[0].astype(jnp.float32)).astype(jnp.bfloat16)
        c0 = send(keep.at[0, theirs], r2.at[theirs], rs_send.at[k, 2], rs_recv.at[k, 2], x_peer)
        c1 = send(keep.at[0, mine], r2.at[mine], rs_send.at[k, 3], rs_recv.at[k, 3], x_peer)
        b.wait_recv()
        hooks[1]()
        c0.wait_recv()

        def total(where):
            return (
                s[where, span(t, feats)].astype(jnp.float32)
                + r1[1, where, :].astype(jnp.float32)
                + r2[where, :].astype(jnp.float32)
            )

        s3[...] = total(theirs).astype(jnp.bfloat16)
        e = send(s3, r3, rs_send.at[k, 4], rs_recv.at[k, 4], (fz[1], t))
        c1.wait_recv()
        part = total(mine)
        hooks[2]()
        e.wait_recv()
        out[...] = (base[...].astype(jnp.float32) + (part + r3[...].astype(jnp.float32))).astype(jnp.bfloat16)

    def finish(k, acts, weight, s, r1, keep, r2, s3, r3, base, out):
        core_peer, x_peer, z_peer = (f, t_core), (f, t_x), (fz[1], t)
        low, high = pl.ds(0, cut), pl.ds(cut, feats - cut)

        def project(block):
            at = span(block, feats)
            s[:, at] = jnp.dot(acts[...], weight[:, at], preferred_element_type=jnp.float32).astype(jnp.bfloat16)
            return s.at[:, at]

        def go(i, src, dst, peer):
            return send(src, dst, rs_send.at[k, i], rs_recv.at[k, i], peer)

        def pair_sum(block, i):
            return s[:, span(block, feats)].astype(jnp.float32) + r1[i].astype(jnp.float32)

        a = go(0, project(t_xc), r1.at[0], core_peer)
        b = go(1, project(t_core), r1.at[1], core_peer)
        project(t_x)
        project(t)
        a.wait_recv()
        keep[0] = pair_sum(t_x, 0).astype(jnp.bfloat16)
        c = go(2, keep.at[0, :, low], r2.at[:, low], x_peer)
        d = go(3, keep.at[0, theirs, high], r3.at[0, :, high], z_peer)
        b.wait_recv()
        keep[1] = pair_sum(t, 1).astype(jnp.bfloat16)
        e = go(4, keep.at[1, theirs, high], r3.at[1, :, high], z_peer)
        d.wait_recv()
        s3[:, high] = (
            keep[0, mine, high].astype(jnp.float32) + r3[0, :, high].astype(jnp.float32)
        ).astype(jnp.bfloat16)
        g = go(5, s3.at[:, high], r2.at[pl.ds(0, rows), high], x_peer)
        c.wait_recv()
        s3[:, low] = (
            keep[1, theirs, low].astype(jnp.float32) + r2[theirs, low].astype(jnp.float32)
        ).astype(jnp.bfloat16)
        l = go(6, s3.at[:, low], r3.at[0, :, low], z_peer)
        e.wait_recv()
        g.wait_recv()
        out[:, high] = (
            base[:, high].astype(jnp.float32)
            + (keep[1, mine, high].astype(jnp.float32) + r3[1, :, high].astype(jnp.float32))
            + r2[pl.ds(0, rows), high].astype(jnp.float32)
        ).astype(jnp.bfloat16)
        l.wait_recv()
        out[:, low] = (
            base[:, low].astype(jnp.float32)
            + (keep[1, mine, low].astype(jnp.float32) + r2[mine, low].astype(jnp.float32))
            + r3[0, :, low].astype(jnp.float32)
        ).astype(jnp.bfloat16)

    def forwards(*pairs):
        def go():
            for group, d in pairs:
                forward(group, d)

        return go

    state = gather_start(0, tok, x1)
    for group in range(5):
        launch(group)
    if fill:
        for w in (wgate, wup, wdn):
            w[pl.ds(half_ff, fill), :] = jnp.zeros((fill, model), jnp.bfloat16)
    gather_rest(state, (forwards((0, 1), (1, 1)), forwards((0, 2), (1, 2)), forwards((0, 3), (1, 3))))
    norm(x1, gain1, nb)
    forwards((2, 1), (2, 2), (2, 3))()
    arrive(0)
    arrive(1)
    forward(3, 1)
    both = jnp.dot(nb[...], win[...], preferred_element_type=jnp.float32)
    branch_in, branch_gate = both[:, :LANES], both[:, LANES:]
    row = lax.broadcasted_iota(jnp.int32, branch_in.shape, 0)
    pos = jnp.where(row >= rows, row - rows, row)

    def shifted(values, by, fill):
        return jnp.where(pos >= by, pltpu.roll(values, by, 0), fill)

    tap_count = taps.shape[0]
    my = span(h, LANES)
    conv = branch_in * taps[tap_count - 1 :, my]
    for j in range(tap_count - 1):
        conv = conv + shifted(branch_in, tap_count - 1 - j, 0.0) * taps[j : j + 1, my]
    conv = conv.astype(jnp.bfloat16)
    gate_x = jax.nn.sigmoid(jnp.dot(conv, gxb[h], preferred_element_type=jnp.float32))
    gate_a = jax.nn.sigmoid(jnp.dot(conv, gab[h], preferred_element_type=jnp.float32))
    log_decay = -gate_power * gate_a * forget[:, my]
    decay = jnp.exp(log_decay)
    scale = jnp.sqrt(-jnp.tanh(log_decay) * (1.0 + decay * decay))
    scale = jnp.where(pos == 0, 1.0, scale)
    run = conv.astype(jnp.float32) * gate_x * scale
    by = 1
    while by < rows:
        run = decay * shifted(run, by, 0.0) + run
        decay = decay * shifted(decay, by, 1.0)
        by *= 2
    mix[...] = (run * jax.nn.gelu(branch_gate)).astype(jnp.bfloat16)
    arrive(2)
    forward(3, 2)
    scatter(
        0, mix, wout, s1, s1r, k1, x1r, zs1, z1r, tok, after,
        (forwards((3, 3)), forwards((4, 1)), forwards((4, 2))),
    )
    state = gather_start(1, after, x2)
    launch(5)
    gather_rest(state, (forwards((4, 3)), forwards(), forwards((5, 1))))
    norm(x2, gain2, nb)
    forward(5, 2)
    arrive(3)
    arrive(4)
    forward(5, 3)
    last = (((1,), (1,)), ((), ()))

    def ffn(i, carry):
        at = span(i, LANES)
        gate_val = lax.dot_general(nb[...], wgate[at, :], last, preferred_element_type=jnp.float32)
        up_val = lax.dot_general(nb[...], wup[at, :], last, preferred_element_type=jnp.float32)
        hid[:, at] = (jax.nn.silu(gate_val) * up_val).astype(jnp.bfloat16)
        return carry

    lax.fori_loop(0, wgate.shape[0] // LANES, ffn, 0)
    arrive(5)
    finish(1, hid, wdn, s2, s2r, k2, x2r, zs2, z2r, after, result)
    for copy in started:
        copy.wait_send()


def on_device_paired(
    tokens, mix_gain, in_x_w, in_gate_w, conv_taps, gate_x_blocks, gate_a_blocks, forget_rate,
    out_w, ffn_gain, ffn_gate_w, ffn_up_w, ffn_down_w,
):
    rows, feats = tokens.shape
    model = mix_gain.shape[0]
    both = 2 * rows
    wide = -(-ffn_down_w.shape[0] // (2 * LANES)) * LANES
    bf, dma = jnp.bfloat16, pltpu.SemaphoreType.DMA
    exchange = [
        pltpu.VMEM((both, model), bf),
        pltpu.VMEM((2, both, feats), bf),
        pltpu.VMEM((2, both, feats), bf),
        pltpu.VMEM((both, feats), bf),
    ]
    vmem = pl.BlockSpec(memory_space=pltpu.VMEM)
    return pl.pallas_call(
        kernel,
        out_shape=jax.ShapeDtypeStruct((rows, feats), bf),
        in_specs=[vmem] * 13,
        out_specs=vmem,
        scratch_shapes=[
            pltpu.VMEM((both, model), bf),
            pltpu.VMEM((both, model), bf),
            pltpu.VMEM((model, 2 * LANES), bf),
            pltpu.VMEM((LANES, model), bf),
            pltpu.VMEM((wide, model), bf),
            pltpu.VMEM((wide, model), bf),
            pltpu.VMEM((wide, model), bf),
            *exchange,
            pltpu.VMEM((rows, feats), bf),
            pltpu.VMEM((rows, feats), bf),
            pltpu.VMEM((rows, feats), bf),
            pltpu.VMEM((both, LANES), bf),
            pltpu.VMEM((both, model), bf),
            pltpu.VMEM((both, wide), bf),
            *exchange,
            pltpu.VMEM((rows, feats), bf),
            pltpu.VMEM((2, rows, feats), bf),
            dma((6, 3)), dma((6, 3)), dma((6, 4)), dma((6, 4)), dma((6,)),
            dma((2, 7)), dma((2, 7)), dma((2, 7)), dma((2, 7)),
        ],
        compiler_params=pltpu.CompilerParams(
            collective_id=0, has_side_effects=True, vmem_limit_bytes=48 * 1024 * 1024
        ),
    )(
        tokens, mix_gain.reshape(1, model), in_x_w, in_gate_w, conv_taps, gate_x_blocks, gate_a_blocks,
        forget_rate.reshape(1, -1), out_w, ffn_gain.reshape(1, model), ffn_gate_w.T, ffn_up_w.T, ffn_down_w,
    )


def solution(mesh):
    def body(*args):
        if paired(mesh, *args):
            return on_device_paired(*args)
        return on_device(*args)

    placed = (
        P("fs", "tp"),
        P(),
        P("fs", "tp"),
        P("fs", "tp"),
        P(None, "tp"),
        P("tp", None, None),
        P("tp", None, None),
        P("tp"),
        P("tp", "fs"),
        P(),
        P("fs", "tp"),
        P("fs", "tp"),
        P("tp", "fs"),
    )
    return jax.shard_map(
        body, mesh=mesh, in_specs=placed, out_specs=P("fs", "tp"), check_vma=False
    )
```

profile of v0, /device:TPU:0, one launch (start us, length us, event | category | flops | bytes accessed | tf_op | source)
XLA Modules:
  0.0 103.2 jit_solution(15580444332802014514)
XLA Ops:
  0.0 0.0 copy-start.9
  0.0 0.0 copy-start.12
  0.0 0.7 copy-done.9
  0.7 0.0 copy-done.12
  0.7 0.0 copy-start
  0.7 1.0 copy-done
  1.7 0.0 copy-start.1
  1.7 1.0 copy-done.1
  2.7 0.0 copy-start.2
  2.7 1.0 copy-done.2
  3.7 0.0 copy-start.3
  3.7 0.9 copy-done.3
  4.6 0.0 copy-start.4
  4.6 0.9 copy-done.4
  5.5 0.0 copy-start.5
  5.5 0.9 copy-done.5
  6.4 0.0 copy-start.6
  6.4 0.9 copy-done.6
  7.3 0.0 copy-start.7
  7.3 0.8 copy-done.7
  8.1 0.0 copy-start.8
  8.1 0.8 copy-done.8
  9.0 0.0 copy-start.10
  9.0 0.7 copy-done.10
  9.7 0.0 copy-start.11
  9.7 0.7 copy-done.11
  10.4 92.1 %shard_map.127 = bf16[160,512]{1,0:T(8,128)(2,1)S(1)} custom-call(bf16[160,512]{1,0:T(8,128)(2,1)S(1)} %copy-done.3, f32[1,2048]{1,0:T(1,128)S(1)} %bitcast.7, bf16[256,256]{1,0:T(8,128)(2,1)S(1)} %copy-done.4, bf16[256,256]{1,0:T(8,128)(2,1)S(1)} %copy-done.5, f32[4,256]{1,0:T(4,128)S(1)} %copy-done.11, bf16[2,128,128]{2,1,0:T(8,128)(2,1)S(1)} %copy-done.7, ...), custom_call_target="tpu_custom_call" | custom-call | tf_op jit(solution)/shard_map/pallas_call | solution.py:426
  102.5 0.7 copy.15
Async XLA Ops:
  0.0 0.7 copy-start.9
  0.0 0.7 copy-start.12
  0.7 1.0 copy-start
  1.7 1.0 copy-start.1
  2.7 1.0 copy-start.2
  3.7 0.9 copy-start.3
  4.6 0.9 copy-start.4
  5.5 0.9 copy-start.5
  6.4 0.9 copy-start.6
  7.3 0.8 copy-start.7
  8.1 0.8 copy-start.8
  9.0 0.7 copy-start.10
  9.7 0.7 copy-start.11
where the time goes:
time: 104 us; the launch traced here: 103 us
  Pallas kernels  92.1 us (89%)
  local copies, waits for them, and re-layouts  11 us (11%)
    pallas_call x1, Pallas kernels, on_device_paired(): pl.pallas_call(kernel, out_shape=jax.ShapeDtypeStruct((rows, feats), bf),...  92.1 us
    unnamed x27, local copies, waits for them, and re-layouts  11 us

commit v1 on v0

--- a/solution.py
+++ b/solution.py
@@ -120,8 +120,9 @@
 
 
 def kernel(
-    tok, gain1, w_x, w_g, taps, gxb, gab, forget, w_out, gain2, w_gate, w_up, w_dn,
+    h_tok, h_gain1, h_x, h_g, h_taps, h_gxb, h_gab, h_forget, h_out, h_gain2, h_gate, h_up, h_dn,
     result,
+    tok, gain1, w_x, w_g, taps, gxb, gab, forget, w_out, gain2, w_gate, w_up, w_dn, load_sem,
     x1, nb, win, wout, wgate, wup, wdn, s1, s1r, k1, x1r, zs1, z1r, after, mix, x2, hid,
     s2, s2r, k2, x2r, zs2, z2r,
     send_z, recv_z, send_y, recv_y, own_sem, ag_send, ag_recv, rs_send, rs_recv,
@@ -138,6 +139,12 @@
     t_xc = (t_core + 2) % 4
     model = x1.shape[1]
 
+    held = (tok, w_x, w_g, w_out, w_gate, w_up, w_dn, gain1, taps, gxb, gab, forget, gain2)
+    given = (h_tok, h_x, h_g, h_out, h_gate, h_up, h_dn, h_gain1, h_taps, h_gxb, h_gab, h_forget, h_gain2)
+    loads = [pltpu.make_async_copy(src, dst, load_sem.at[i]) for i, (src, dst) in enumerate(zip(given, held))]
+    for load in loads:
+        load.start()
+
     barrier = pltpu.get_barrier_semaphore()
     peers = [(fz[1], t), (fz[2], t), (fz[3], t), (fy, t), (f, t_core), (f, t_x)]
     for peer in peers:
@@ -163,12 +170,12 @@
     half_ff = w_dn.shape[0] // 2
     fill = wdn.shape[0] - half_ff
 
-    def piece(group, half):
+    def piece(group, half, stored=False):
         if group < 2:
-            return (w_x, w_g)[group].at[:, span(half, LANES)]
+            return ((h_x, h_g) if stored else (w_x, w_g))[group].at[:, span(half, LANES)]
         if group == 2:
-            return w_out.at[span(half, LANES), :]
-        return (w_gate, w_up, w_dn)[group - 3].at[span(half, half_ff), :]
+            return (h_out if stored else w_out).at[span(half, LANES), :]
+        return ((h_gate, h_up, h_dn) if stored else (w_gate, w_up, w_dn))[group - 3].at[span(half, half_ff), :]
 
     def place(group, source):
         if group < 2:
@@ -180,6 +187,10 @@
     own_copies = {}
     z_copies = {}
     y_copies = {}
+
+    for group in range(6):
+        own_copies[group] = pltpu.make_async_copy(piece(group, h, True), place(group, f), own_sem.at[group])
+        own_copies[group].start()
 
     def launch(group):
         for d in (1, 2, 3):
@@ -191,8 +202,6 @@
                 y_copies[group, 0] = send(
                     piece(group, h), place(group, f), send_y.at[group, 0], recv_y.at[group, 0], (fy, t)
                 )
-        own_copies[group] = pltpu.make_async_copy(piece(group, h), place(group, f), own_sem.at[group])
-        own_copies[group].start()
 
     def forward(group, d):
         z_copies[group, d].wait_recv()
@@ -338,9 +347,13 @@
 
         return go
 
+    loads[0].wait()
     state = gather_start(0, tok, x1)
     for group in range(5):
+        loads[1 + group].wait()
         launch(group)
+    for load in loads[6:]:
+        load.wait()
     if fill:
         for w in (wgate, wup, wdn):
             w[pl.ds(half_ff, fill), :] = jnp.zeros((fill, model), jnp.bfloat16)
@@ -423,12 +436,18 @@
         pltpu.VMEM((both, feats), bf),
     ]
     vmem = pl.BlockSpec(memory_space=pltpu.VMEM)
+    operands = (
+        tokens, mix_gain.reshape(1, model), in_x_w, in_gate_w, conv_taps, gate_x_blocks, gate_a_blocks,
+        forget_rate.reshape(1, -1), out_w, ffn_gain.reshape(1, model), ffn_gate_w.T, ffn_up_w.T, ffn_down_w,
+    )
     return pl.pallas_call(
         kernel,
         out_shape=jax.ShapeDtypeStruct((rows, feats), bf),
-        in_specs=[vmem] * 13,
+        in_specs=[pl.BlockSpec(memory_space=pltpu.HBM)] * 13,
         out_specs=vmem,
         scratch_shapes=[
+            *[pltpu.VMEM(operand.shape, operand.dtype) for operand in operands],
+            dma((13,)),
             pltpu.VMEM((both, model), bf),
             pltpu.VMEM((both, model), bf),
             pltpu.VMEM((model, 2 * LANES), bf),
@@ -450,12 +469,9 @@
             dma((2, 7)), dma((2, 7)), dma((2, 7)), dma((2, 7)),
         ],
         compiler_params=pltpu.CompilerParams(
-            collective_id=0, has_side_effects=True, vmem_limit_bytes=48 * 1024 * 1024
+            collective_id=0, has_side_effects=True, vmem_limit_bytes=64 * 1024 * 1024 - 64 * 1024
         ),
-    )(
-        tokens, mix_gain.reshape(1, model), in_x_w, in_gate_w, conv_taps, gate_x_blocks, gate_a_blocks,
-        forget_rate.reshape(1, -1), out_w, ffn_gain.reshape(1, model), ffn_gate_w.T, ffn_up_w.T, ffn_down_w,
-    )
+    )(*operands)
 
 
 def solution(mesh):

time: 104 us -> 94.7 us (0.911)
  local copies, waits for them, and re-layouts: 11 us -> 1.59 us
    unnamed x27 -> x1, local copies, waits for them, and re-layouts: 11 us -> 1.59 us
where the time goes in v1:
time: 94.7 us; the launch traced here: 94.5 us
  Pallas kernels  92.9 us (98%)
  local copies, waits for them, and re-layouts  1.59 us (2%)
    pallas_call x1, Pallas kernels, on_device_paired(): pl.pallas_call(kernel, out_shape=jax.ShapeDtypeStruct((rows, feats), bf),...  92.9 us

profile of v1, /device:TPU:0, one launch (start us, length us, event | category | flops | bytes accessed | tf_op | source)
XLA Modules:
  0.0 94.5 jit_solution(12298333961616702118)
XLA Ops:
  0.0 92.9 %shard_map.127 = bf16[160,512]{1,0:T(8,128)(2,1)} custom-call(bf16[160,512]{1,0:T(8,128)(2,1)} %h_tok.1, f32[1,2048]{1,0:T(1,128)} %bitcast.7, bf16[256,256]{1,0:T(8,128)(2,1)} %h_x.1, bf16[256,256]{1,0:T(8,128)(2,1)} %h_g.1, f32[4,256]{1,0:T(4,128)} %h_taps.1, bf16[2,128,128]{2,1,0:T(8,128)(2,1)} %h_gxb.1, bf16[2,128,128]{2,1,0:T(8,128)(2,1)} %h_gab.1, ...), custom_call_target="tpu_custom_call" | custom-call | tf_op jit(solution)/shard_map/pallas_call | solution.py:443
  92.9 1.6 %copy.15 = bf16[160,512]{1,0:T(8,128)(2,1)} copy(bf16[160,512]{1,0:T(8,128)(2,1)} %shard_map.127) | data formatting | bytes 327680

commit v2 on v1

--- a/solution.py
+++ b/solution.py
@@ -113,10 +113,14 @@
         mesh.shape["fs"] == 8
         and mesh.shape["tp"] == 4
         and gate_x_blocks.shape == (2, LANES, LANES)
-        and tokens.shape[0] % 16 == 0
-        and tokens.shape[1] % (2 * LANES) == 0
+        and tokens.shape[0] % 32 == 0
+        and tokens.shape[1] == 4 * LANES
+        and ffn_down_w.shape[1] == 2 * LANES
         and ffn_down_w.shape[0] % 32 == 0
     )
+
+
+PARTS = 2
 
 
 def kernel(
@@ -125,19 +129,25 @@
     tok, gain1, w_x, w_g, taps, gxb, gab, forget, w_out, gain2, w_gate, w_up, w_dn, load_sem,
     x1, nb, win, wout, wgate, wup, wdn, s1, s1r, k1, x1r, zs1, z1r, after, mix, x2, hid,
     s2, s2r, k2, x2r, zs2, z2r,
-    send_z, recv_z, send_y, recv_y, own_sem, ag_send, ag_recv, rs_send, rs_recv,
+    send_z, recv_z, send_y, recv_y, own_sem, ag_send, ag_recv, rs_send, rs_recv, fin_send, fin_recv,
 ):
     f, t = lax.axis_index("fs"), lax.axis_index("tp")
     z, y = f // 2, f % 2
     h = z % 2
+    outer = (z == 0) | (z == 3)
+    inner = (z == 1) | (z == 2)
     rows, feats = tok.shape
-    zs = (z, z + 1 - 2 * h, (z + 2) % 4, 3 - z)
-    fz = tuple(zz * 2 + y for zz in zs)
+    near_z = z + 1 - 2 * h
+    far_outer = 3 * (1 - z // 2)
+    far_inner = 2 - z // 2
+    sources = (z, near_z, far_outer, far_inner)
+    fz = tuple(zz * 2 + y for zz in sources)
     fy = z * 2 + 1 - y
     t_core = t + 1 - 2 * (t % 2)
     t_x = (t + 2) % 4
     t_xc = (t_core + 2) % 4
     model = x1.shape[1]
+    scope = jax.named_scope
 
     held = (tok, w_x, w_g, w_out, w_gate, w_up, w_dn, gain1, taps, gxb, gab, forget, gain2)
     given = (h_tok, h_x, h_g, h_out, h_gate, h_up, h_dn, h_gain1, h_taps, h_gxb, h_gab, h_forget, h_gain2)
@@ -149,15 +159,19 @@
     peers = [(fz[1], t), (fz[2], t), (fz[3], t), (fy, t), (f, t_core), (f, t_x)]
     for peer in peers:
         pl.semaphore_signal(barrier, inc=1, device_id=peer, device_id_type=pl.DeviceIdType.MESH)
-    pl.semaphore_wait(barrier, len(peers))
+    with scope("barrier"):
+        pl.semaphore_wait(barrier, len(peers))
 
     started = []
 
-    def send(src, dst, s_sem, r_sem, peer):
-        copy = pltpu.make_async_remote_copy(
+    def describe(src, dst, s_sem, r_sem, peer):
+        return pltpu.make_async_remote_copy(
             src_ref=src, dst_ref=dst, send_sem=s_sem, recv_sem=r_sem,
             device_id=peer, device_id_type=pl.DeviceIdType.MESH,
         )
+
+    def send(src, dst, s_sem, r_sem, peer):
+        copy = describe(src, dst, s_sem, r_sem, peer)
         copy.start()
         started.append(copy)
         return copy
@@ -167,80 +181,141 @@
 
     depth = w_x.shape[0]
     cols = w_out.shape[1]
+    part_cols = cols // PARTS
     half_ff = w_dn.shape[0] // 2
-    fill = wdn.shape[0] - half_ff
+    fill = wgate.shape[0] - half_ff
+    last_group = 4 + PARTS
 
     def piece(group, half, stored=False):
         if group < 2:
             return ((h_x, h_g) if stored else (w_x, w_g))[group].at[:, span(half, LANES)]
         if group == 2:
             return (h_out if stored else w_out).at[span(half, LANES), :]
-        return ((h_gate, h_up, h_dn) if stored else (w_gate, w_up, w_dn))[group - 3].at[span(half, half_ff), :]
+        if group < 5:
+            return ((h_gate, h_up) if stored else (w_gate, w_up))[group - 3].at[span(half, half_ff), :]
+        return (h_dn if stored else w_dn).at[span(half, half_ff), pl.ds((group - 5) * part_cols, part_cols)]
 
     def place(group, source):
         if group < 2:
             return win.at[span(source, depth), pl.ds(group * LANES, LANES)]
         if group == 2:
             return wout.at[:, span(source, cols)]
-        return (wgate, wup, wdn)[group - 3].at[pl.ds(0, half_ff), span(source, cols)]
-
+        if group < 5:
+            return (wgate, wup)[group - 3].at[pl.ds(0, half_ff), span(source, cols)]
+        return wdn.at[group - 5, pl.ds(0, half_ff), span(source, part_cols)]
+
+    groups = range(last_group + 1)
     own_copies = {}
-    z_copies = {}
-    y_copies = {}
-
-    for group in range(6):
+    for group in groups:
         own_copies[group] = pltpu.make_async_copy(piece(group, h, True), place(group, f), own_sem.at[group])
         own_copies[group].start()
 
-    def launch(group):
-        for d in (1, 2, 3):
-            half = h if d == 2 else 1 - h
-            z_copies[group, d] = send(
-                piece(group, half), place(group, f), send_z.at[group, d - 1], recv_z.at[group, d - 1], (fz[d], t)
+    slot = jnp.where(outer, 2, 3)
+    z_sends = {}
+    for group in groups:
+        for way, peer in ((1, fz[1]), (2, fz[2]), (3, fz[3])):
+            half = (1 - h, far_outer % 2, far_inner % 2)[way - 1]
+            at = 1 if way == 1 else slot
+            z_sends[group, way] = describe(
+                piece(group, half), place(group, f), send_z.at[group, way - 1], recv_z.at[group, at - 1], (peer, t)
             )
-            if d == 1:
-                y_copies[group, 0] = send(
-                    piece(group, h), place(group, f), send_y.at[group, 0], recv_y.at[group, 0], (fy, t)
-                )
+            if way != 2:
+                started.append(z_sends[group, way])
+    y_copies, relays = {}, {}
+
+    after_relay = {0: (2,), 2: (3,), 3: (4,), 4: (5, 6)}
+
+    def near(*names):
+        for group in names:
+            z_sends[group, 1].start()
+
+    def far(*names):
+        @pl.when(outer)
+        def _():
+            for group in names:
+                z_sends[group, 3].start()
+
+    def y_own(*names):
+        for group in names:
+            y_copies[group, 0] = send(
+                piece(group, h), place(group, f), send_y.at[group, 0], recv_y.at[group, 0], (fy, t)
+            )
+
+    def pick(when_inner, when_outer):
+        return jnp.where(inner, when_inner, when_outer)
+
+    arrival = (pick(1, 3), pick(2, 1), pick(3, 2))
+    arrival_fz = (pick(fz[1], fz[3]), pick(fz[2], fz[1]), pick(fz[3], fz[2]))
 
     def forward(group, d):
-        z_copies[group, d].wait_recv()
-        y_copies[group, d] = send(
-            place(group, fz[d]), place(group, fz[d]), send_y.at[group, d], recv_y.at[group, d], (fy, t)
-        )
+        block = place(group, arrival_fz[d - 1])
+        describe(
+            block, block, send_z.at[group, 0], recv_z.at[group, arrival[d - 1] - 1], (fz[1], t)
+        ).wait_recv()
+        y_copies[group, d] = send(block, block, send_y.at[group, d], recv_y.at[group, d], (fy, t))
+        if d == 1:
+            relays[group] = describe(block, block, send_z.at[group, 3], recv_z.at[group, 1], (fz[2], t))
+
+            @pl.when(inner)
+            def _():
+                relays[group].start()
+                for next_group in after_relay.get(group, ()):
+                    z_sends[next_group, 2].start()
+                    z_sends[next_group, 3].start()
 
     def arrive(group):
         own_copies[group].wait()
         for d in range(4):
             y_copies[group, d].wait_recv()
 
-    cut = feats // 2
     mine, theirs = span(h, rows), span(1 - h, rows)
+    cut = rows // 2
+
+    def some(block, c):
+        return pl.ds(pl.multiple_of(block * rows + c * cut, cut), cut)
 
     def gather_start(k, own, x):
-        def go(i, r, c, peer):
-            src = own if i < 3 else x.at[r, span(c, feats)]
-            return send(src, x.at[r, span(c, feats)], ag_send.at[k, i], ag_recv.at[k, i], peer)
-
         x_peer, core_peer = (f, t_x), (f, t_core)
-        first = go(0, mine, t, (fz[1], t)), go(1, mine, t, x_peer), go(2, mine, t, core_peer)
-        x[mine, span(t, feats)] = own[...]
-        return go, first, x_peer, core_peer
-
-    def gather_rest(state, hooks):
-        go, (by_z, by_x, by_core), x_peer, core_peer = state
-        by_z.wait_recv()
-        c3 = go(3, theirs, t, x_peer)
-        c4 = go(4, theirs, t, core_peer)
-        hooks[0]()
-        by_x.wait_recv()
-        c5 = go(5, mine, t_x, core_peer)
-        hooks[1]()
-        c3.wait_recv()
-        c6 = go(6, theirs, t_x, core_peer)
-        hooks[2]()
-        for c in (by_core, c4, c5, c6):
-            c.wait_recv()
+
+        def go(i, src, dst, peer):
+            return send(src, dst, ag_send.at[k, i], ag_recv.at[k, i], peer)
+
+        at = span(t, feats)
+        by_z = [go(c, own.at[pl.ds(c * cut, cut), :], x.at[some(h, c), at], (fz[1], t)) for c in range(2)]
+        by_x = go(2, own, x.at[mine, at], x_peer)
+        by_core = go(3, own, x.at[mine, at], core_peer)
+        x[mine, at] = own[...]
+        return go, by_z, by_x, by_core, x_peer, core_peer, x
+
+    def gather_relay(state):
+        go, by_z, by_x, by_core, x_peer, core_peer, x = state
+        across, inside = [], [by_core]
+        at = span(t, feats)
+        with scope("byz"):
+            for c in range(2):
+                by_z[c].wait_recv()
+                block = x.at[some(1 - h, c), at]
+                across.append(go(4 + c, block, block, x_peer))
+                inside.append(go(6 + c, block, block, core_peer))
+        with scope("byx"):
+            by_x.wait_recv()
+        block = x.at[mine, span(t_x, feats)]
+        inside.append(go(8, block, block, core_peer))
+        return across, inside
+
+    def gather_pass(state, relayed):
+        go, core_peer, x = state[0], state[5], state[6]
+        across, inside = relayed
+        with scope("across"):
+            for c in range(2):
+                across[c].wait_recv()
+                block = x.at[some(1 - h, c), span(t_x, feats)]
+                inside.append(go(9 + c, block, block, core_peer))
+
+    def gather_end(relayed):
+        with scope("inside"):
+            for copy in relayed[1]:
+                copy.wait_recv()
 
     def norm(x, gain, out):
         step = 32
@@ -266,14 +341,19 @@
         b = send(project(t_core), r1.at[1], rs_send.at[k, 1], rs_recv.at[k, 1], core_peer)
         project(t_x)
         project(t)
+        with scope("rs_a"):
+            a.wait_recv()
+        at = span(t_x, feats)
+        for i, block in ((0, theirs), (1, mine)):
+            keep[0, block, :] = (s[block, at].astype(jnp.float32) + r1[0, block, :].astype(jnp.float32)).astype(jnp.bfloat16)
+            copy = send(keep.at[0, block], r2.at[block], rs_send.at[k, 2 + i], rs_recv.at[k, 2 + i], x_peer)
+            if i == 0:
+                c0 = copy
+        c1 = copy
         hooks[0]()
-        a.wait_recv()
-        keep[0] = (s[:, span(t_x, feats)].astype(jnp.float32) + r1[0].astype(jnp.float32)).astype(jnp.bfloat16)
-        c0 = send(keep.at[0, theirs], r2.at[theirs], rs_send.at[k, 2], rs_recv.at[k, 2], x_peer)
-        c1 = send(keep.at[0, mine], r2.at[mine], rs_send.at[k, 3], rs_recv.at[k, 3], x_peer)
-        b.wait_recv()
-        hooks[1]()
-        c0.wait_recv()
+        with scope("rs_c0"):
+            b.wait_recv()
+            c0.wait_recv()
 
         def total(where):
             return (
@@ -284,85 +364,133 @@
 
         s3[...] = total(theirs).astype(jnp.bfloat16)
         e = send(s3, r3, rs_send.at[k, 4], rs_recv.at[k, 4], (fz[1], t))
-        c1.wait_recv()
+        hooks[1]()
+        with scope("rs_c1"):
+            c1.wait_recv()
         part = total(mine)
         hooks[2]()
-        e.wait_recv()
+        with scope("rs_e"):
+            e.wait_recv()
         out[...] = (base[...].astype(jnp.float32) + (part + r3[...].astype(jnp.float32))).astype(jnp.bfloat16)
 
-    def finish(k, acts, weight, s, r1, keep, r2, s3, r3, base, out):
+    def finish(p, acts):
         core_peer, x_peer, z_peer = (f, t_core), (f, t_x), (fz[1], t)
-        low, high = pl.ds(0, cut), pl.ds(cut, feats - cut)
+        wide = feats // PARTS
+        low, high = pl.ds(0, wide // 2), pl.ds(wide // 2, wide // 2)
+        s, r1, keep, r2, s3, r3 = s2.at[p], s2r.at[p], k2.at[p], x2r.at[p], zs2.at[p], z2r.at[p]
 
         def project(block):
-            at = span(block, feats)
-            s[:, at] = jnp.dot(acts[...], weight[:, at], preferred_element_type=jnp.float32).astype(jnp.bfloat16)
+            at = span(block, wide)
+            s[:, at] = jnp.dot(acts[...], wdn[p, :, at], preferred_element_type=jnp.float32).astype(jnp.bfloat16)
             return s.at[:, at]
 
         def go(i, src, dst, peer):
-            return send(src, dst, rs_send.at[k, i], rs_recv.at[k, i], peer)
+            return send(src, dst, fin_send.at[p, i], fin_recv.at[p, i], peer)
 
         def pair_sum(block, i):
-            return s[:, span(block, feats)].astype(jnp.float32) + r1[i].astype(jnp.float32)
+            return s[:, span(block, wide)].astype(jnp.float32) + r1[i].astype(jnp.float32)
 
         a = go(0, project(t_xc), r1.at[0], core_peer)
         b = go(1, project(t_core), r1.at[1], core_peer)
         project(t_x)
         project(t)
-        a.wait_recv()
-        keep[0] = pair_sum(t_x, 0).astype(jnp.bfloat16)
-        c = go(2, keep.at[0, :, low], r2.at[:, low], x_peer)
-        d = go(3, keep.at[0, theirs, high], r3.at[0, :, high], z_peer)
-        b.wait_recv()
-        keep[1] = pair_sum(t, 1).astype(jnp.bfloat16)
-        e = go(4, keep.at[1, theirs, high], r3.at[1, :, high], z_peer)
-        d.wait_recv()
-        s3[:, high] = (
-            keep[0, mine, high].astype(jnp.float32) + r3[0, :, high].astype(jnp.float32)
-        ).astype(jnp.bfloat16)
-        g = go(5, s3.at[:, high], r2.at[pl.ds(0, rows), high], x_peer)
-        c.wait_recv()
-        s3[:, low] = (
-            keep[1, theirs, low].astype(jnp.float32) + r2[theirs, low].astype(jnp.float32)
-        ).astype(jnp.bfloat16)
-        l = go(6, s3.at[:, low], r3.at[0, :, low], z_peer)
-        e.wait_recv()
-        g.wait_recv()
-        out[:, high] = (
-            base[:, high].astype(jnp.float32)
-            + (keep[1, mine, high].astype(jnp.float32) + r3[1, :, high].astype(jnp.float32))
-            + r2[pl.ds(0, rows), high].astype(jnp.float32)
-        ).astype(jnp.bfloat16)
-        l.wait_recv()
-        out[:, low] = (
-            base[:, low].astype(jnp.float32)
-            + (keep[1, mine, low].astype(jnp.float32) + r2[mine, low].astype(jnp.float32))
-            + r3[0, :, low].astype(jnp.float32)
-        ).astype(jnp.bfloat16)
+        waits = {}
+
+        def cross():
+            with scope(f"fin_a{p}"):
+                a.wait_recv()
+            keep[0] = pair_sum(t_x, 0).astype(jnp.bfloat16)
+            waits["d"] = go(3, keep.at[0, theirs, high], r3.at[0, :, high], z_peer)
+            waits["c"] = go(2, keep.at[0, theirs, low], r2.at[theirs, low], x_peer)
+            waits["m"] = go(7, keep.at[0, mine, low], r2.at[mine, low], x_peer)
+            with scope(f"fin_b{p}"):
+                b.wait_recv()
+            keep[1] = pair_sum(t, 1).astype(jnp.bfloat16)
+            waits["e"] = go(4, keep.at[1, theirs, high], r3.at[1, :, high], z_peer)
+
+        def turn():
+            with scope(f"fin_d{p}"):
+                waits["d"].wait_recv()
+            s3[:, high] = (
+                keep[0, mine, high].astype(jnp.float32) + r3[0, :, high].astype(jnp.float32)
+            ).astype(jnp.bfloat16)
+            waits["g"] = go(5, s3.at[:, high], r2.at[pl.ds(0, rows), high], x_peer)
+            with scope(f"fin_c{p}"):
+                waits["c"].wait_recv()
+            s3[:, low] = (
+                keep[1, theirs, low].astype(jnp.float32) + r2[theirs, low].astype(jnp.float32)
+            ).astype(jnp.bfloat16)
+            waits["l"] = go(6, s3.at[:, low], r3.at[0, :, low], z_peer)
+
+        def end():
+            with scope(f"fin_g{p}"):
+                waits["e"].wait_recv()
+                waits["g"].wait_recv()
+            left, right = pl.ds(p * part_cols, part_cols), pl.ds(cols + p * part_cols, part_cols)
+            result[:, right] = (
+                after[:, right].astype(jnp.float32)
+                + (keep[1, mine, high].astype(jnp.float32) + r3[1, :, high].astype(jnp.float32))
+                + r2[pl.ds(0, rows), high].astype(jnp.float32)
+            ).astype(jnp.bfloat16)
+            with scope(f"fin_l{p}"):
+                waits["m"].wait_recv()
+                waits["l"].wait_recv()
+            result[:, left] = (
+                after[:, left].astype(jnp.float32)
+                + (keep[1, mine, low].astype(jnp.float32) + r2[mine, low].astype(jnp.float32))
+                + r3[0, :, low].astype(jnp.float32)
+            ).astype(jnp.bfloat16)
+
+        return cross, turn, end
 
     def forwards(*pairs):
         def go():
             for group, d in pairs:
-                forward(group, d)
+                with scope(f"fw{group}{d}"):
+                    forward(group, d)
 
         return go
 
-    loads[0].wait()
+    nothing = forwards()
+    for load in loads[:1]:
+        load.wait()
     state = gather_start(0, tok, x1)
-    for group in range(5):
-        loads[1 + group].wait()
-        launch(group)
-    for load in loads[6:]:
+    for load in loads[1:]:
         load.wait()
+    y_own(0, 1)
+
+    for group in range(4):
+        near(group)
+        far(group)
+
+    @pl.when(inner)
+    def _():
+        for group in range(2):
+            z_sends[group, 2].start()
+            z_sends[group, 3].start()
+
+    y_own(2, 3)
     if fill:
-        for w in (wgate, wup, wdn):
+        for w in (wgate, wup):
             w[pl.ds(half_ff, fill), :] = jnp.zeros((fill, model), jnp.bfloat16)
-    gather_rest(state, (forwards((0, 1), (1, 1)), forwards((0, 2), (1, 2)), forwards((0, 3), (1, 3))))
-    norm(x1, gain1, nb)
-    forwards((2, 1), (2, 2), (2, 3))()
-    arrive(0)
-    arrive(1)
-    forward(3, 1)
+        for p in range(PARTS):
+            wdn[p, pl.ds(half_ff, fill), :] = jnp.zeros((fill, wdn.shape[2]), jnp.bfloat16)
+    relayed = gather_relay(state)
+    forwards((0, 1), (0, 2), (0, 3), (1, 1), (1, 2), (1, 3))()
+    gather_pass(state, relayed)
+    forwards((2, 1))()
+    gather_end(relayed)
+    forwards((2, 2))()
+    with scope("norm1"):
+        norm(x1, gain1, nb)
+    forwards((2, 3))()
+    y_own(4)
+    near(4)
+    far(4)
+
+    with scope("arrive01"):
+        arrive(0)
+        arrive(1)
     both = jnp.dot(nb[...], win[...], preferred_element_type=jnp.float32)
     branch_in, branch_gate = both[:, :LANES], both[:, LANES:]
     row = lax.broadcasted_iota(jnp.int32, branch_in.shape, 0)
@@ -390,20 +518,33 @@
         decay = decay * shifted(decay, by, 1.0)
         by *= 2
     mix[...] = (run * jax.nn.gelu(branch_gate)).astype(jnp.bfloat16)
-    arrive(2)
-    forward(3, 2)
-    scatter(
-        0, mix, wout, s1, s1r, k1, x1r, zs1, z1r, tok, after,
-        (forwards((3, 3)), forwards((4, 1)), forwards((4, 2))),
-    )
+    y_own(*groups[5:])
+    with scope("arrive2"):
+        arrive(2)
+
+    def refill():
+        near(5)
+        far(5)
+        forwards((3, 2))()
+
+    scatter(0, mix, wout, s1, s1r, k1, x1r, zs1, z1r, tok, after, (forwards((3, 1)), refill, forwards((3, 3))))
     state = gather_start(1, after, x2)
-    launch(5)
-    gather_rest(state, (forwards((4, 3)), forwards(), forwards((5, 1))))
-    norm(x2, gain2, nb)
-    forward(5, 2)
-    arrive(3)
-    arrive(4)
-    forward(5, 3)
+    near(6)
+    far(6)
+
+    forwards((4, 1), (4, 2))()
+    relayed = gather_relay(state)
+    forwards((4, 3))()
+    gather_pass(state, relayed)
+    forwards((5, 1), (5, 2))()
+    gather_end(relayed)
+    forwards((6, 1))()
+    with scope("norm2"):
+        norm(x2, gain2, nb)
+    forwards((6, 2))()
+    with scope("arrive34"):
+        arrive(3)
+        arrive(4)
     last = (((1,), (1,)), ((), ()))
 
     def ffn(i, carry):
@@ -413,11 +554,30 @@
         hid[:, at] = (jax.nn.silu(gate_val) * up_val).astype(jnp.bfloat16)
         return carry
 
-    lax.fori_loop(0, wgate.shape[0] // LANES, ffn, 0)
-    arrive(5)
-    finish(1, hid, wdn, s2, s2r, k2, x2r, zs2, z2r, after, result)
-    for copy in started:
-        copy.wait_send()
+    with scope("ffn"):
+        lax.fori_loop(0, wgate.shape[0] // LANES, ffn, 0)
+    forwards((5, 3), (6, 3))()
+    with scope("arrive5"):
+        arrive(5)
+    first = finish(0, hid)
+    first[0]()
+    with scope("arrive6"):
+        arrive(6)
+    second = finish(1, hid)
+    second[0]()
+    first[1]()
+    second[1]()
+    first[2]()
+    second[2]()
+    with scope("drain"):
+        for copy in started:
+            copy.wait_send()
+
+        @pl.when(inner)
+        def _():
+            for group in groups:
+                z_sends[group, 2].wait_send()
+                relays[group].wait_send()
 
 
 def on_device_paired(
@@ -427,6 +587,7 @@
     rows, feats = tokens.shape
     model = mix_gain.shape[0]
     both = 2 * rows
+    share = feats // PARTS
     wide = -(-ffn_down_w.shape[0] // (2 * LANES)) * LANES
     bf, dma = jnp.bfloat16, pltpu.SemaphoreType.DMA
     exchange = [
@@ -454,7 +615,7 @@
             pltpu.VMEM((LANES, model), bf),
             pltpu.VMEM((wide, model), bf),
             pltpu.VMEM((wide, model), bf),
-            pltpu.VMEM((wide, model), bf),
+            pltpu.VMEM((PARTS, wide, model // PARTS), bf),
             *exchange,
             pltpu.VMEM((rows, feats), bf),
             pltpu.VMEM((rows, feats), bf),
@@ -462,16 +623,19 @@
             pltpu.VMEM((both, LANES), bf),
             pltpu.VMEM((both, model), bf),
             pltpu.VMEM((both, wide), bf),
-            *exchange,
-            pltpu.VMEM((rows, feats), bf),
-            pltpu.VMEM((2, rows, feats), bf),
-            dma((6, 3)), dma((6, 3)), dma((6, 4)), dma((6, 4)), dma((6,)),
-            dma((2, 7)), dma((2, 7)), dma((2, 7)), dma((2, 7)),
+            pltpu.VMEM((PARTS, both, model // PARTS), bf),
+            pltpu.VMEM((PARTS, 2, both, share), bf),
+            pltpu.VMEM((PARTS, 2, both, share), bf),
+            pltpu.VMEM((PARTS, both, share), bf),
+            pltpu.VMEM((PARTS, rows, share), bf),
+            pltpu.VMEM((PARTS, 2, rows, share), bf),
+            dma((7, 4)), dma((7, 3)), dma((7, 4)), dma((7, 4)), dma((7,)),
+            dma((2, 11)), dma((2, 11)), dma((1, 5)), dma((1, 5)), dma((PARTS, 8)), dma((PARTS, 8)),
         ],
         compiler_params=pltpu.CompilerParams(
-            collective_id=0, has_side_effects=True, vmem_limit_bytes=64 * 1024 * 1024 - 64 * 1024
+            collective_id=0, has_side_effects=True, vmem_limit_bytes=48 * 1024 * 1024
         ),
-    )(*operands)
+    )(*[pltpu.with_memory_space_constraint(operand, pltpu.HBM) for operand in operands])
 
 
 def solution(mesh):

time: 94.7 us -> 88 us (0.929)
  Pallas kernels: 92.9 us -> 87.2 us
    pallas_call x1, Pallas kernels: 92.9 us -> 87.2 us  [on_device_paired(): pl.pallas_call(kernel, out_shape=jax.ShapeDtypeStruct((rows, feats), bf),...]
where the time goes in v2:
time: 88 us; the launch traced here: 87.8 us
  Pallas kernels  87.2 us (99%)
    pallas_call x1, Pallas kernels, on_device_paired(): pl.pallas_call(kernel, out_shape=jax.ShapeDtypeStruct((rows, feats), bf),...  87.2 us

profile of v2, /device:TPU:0, one launch (start us, length us, event | category | flops | bytes accessed | tf_op | source)
XLA Modules:
  0.0 87.8 jit_solution(13529320452848328839)
XLA Ops:
  0.0 87.2 %shard_map.127 = bf16[160,512]{1,0:T(8,128)(2,1)S(1)} custom-call(bf16[160,512]{1,0:T(8,128)(2,1)} %h_tok.1, f32[1,2048]{1,0:T(1,128)} %bitcast.7, bf16[256,256]{1,0:T(8,128)(2,1)} %h_x.1, bf16[256,256]{1,0:T(8,128)(2,1)} %h_g.1, f32[4,256]{1,0:T(4,128)} %h_taps.1, bf16[2,128,128]{2,1,0:T(8,128)(2,1)} %h_gxb.1, bf16[2,128,128]{2,1,0:T(8,128)(2,1)} %h_gab.1, ...), custom_call_target="tpu_custom_call" | custom-call | tf_op jit(solution)/shard_map/pallas_call | solution.py:604
  87.2 0.7 copy.15

commit v3 on v2

--- a/solution.py
+++ b/solution.py
@@ -156,11 +156,20 @@
         load.start()
 
     barrier = pltpu.get_barrier_semaphore()
-    peers = [(fz[1], t), (fz[2], t), (fz[3], t), (fy, t), (f, t_core), (f, t_x)]
+    peers = [(fz[1], t), (fz[3], t), (fy, t), (f, t_core), (f, t_x)]
+
+    def greet(peer):
+        pl.semaphore_signal(barrier, inc=1, device_id=peer, device_id_type=pl.DeviceIdType.MESH)
+
     for peer in peers:
-        pl.semaphore_signal(barrier, inc=1, device_id=peer, device_id_type=pl.DeviceIdType.MESH)
+        greet(peer)
+
+    @pl.when(inner)
+    def _():
+        greet((fz[2], t))
+
     with scope("barrier"):
-        pl.semaphore_wait(barrier, len(peers))
+        pl.semaphore_wait(barrier, len(peers) + jnp.where(inner, 1, 0))
 
     started = []
 
@@ -223,7 +232,9 @@
                 started.append(z_sends[group, way])
     y_copies, relays = {}, {}
 
-    after_relay = {0: (2,), 2: (3,), 3: (4,), 4: (5, 6)}
+    after_relay = {
+        0: ((2, 2), (2, 3)), 2: ((3, 2), (3, 3)), 3: ((4, 2), (4, 3)), 4: ((5, 2), (6, 2), (5, 3)), 6: ((6, 3),),
+    }
 
     def near(*names):
         for group in names:
@@ -244,10 +255,11 @@
     def pick(when_inner, when_outer):
         return jnp.where(inner, when_inner, when_outer)
 
-    arrival = (pick(1, 3), pick(2, 1), pick(3, 2))
-    arrival_fz = (pick(fz[1], fz[3]), pick(fz[2], fz[1]), pick(fz[3], fz[2]))
+    early = (pick(1, 3), pick(2, 1), pick(3, 2)), (pick(fz[1], fz[3]), pick(fz[2], fz[1]), pick(fz[3], fz[2]))
+    late = (1, pick(2, 3), pick(3, 2)), (fz[1], pick(fz[2], fz[3]), pick(fz[3], fz[2]))
 
     def forward(group, d):
+        arrival, arrival_fz = early if group < 5 else late
         block = place(group, arrival_fz[d - 1])
         describe(
             block, block, send_z.at[group, 0], recv_z.at[group, arrival[d - 1] - 1], (fz[1], t)
@@ -259,9 +271,8 @@
             @pl.when(inner)
             def _():
                 relays[group].start()
-                for next_group in after_relay.get(group, ()):
-                    z_sends[next_group, 2].start()
-                    z_sends[next_group, 3].start()
+                for key in after_relay.get(group, ()):
+                    z_sends[key].start()
 
     def arrive(group):
         own_copies[group].wait()
@@ -487,6 +498,11 @@
     y_own(4)
     near(4)
     far(4)
+
+    @pl.when(inner)
+    def _():
+        near(5, 6)
+
 
     with scope("arrive01"):
         arrive(0)
@@ -523,22 +539,23 @@
         arrive(2)
 
     def refill():
-        near(5)
+        @pl.when(outer)
+        def _():
+            near(5, 6)
+
         far(5)
         forwards((3, 2))()
 
     scatter(0, mix, wout, s1, s1r, k1, x1r, zs1, z1r, tok, after, (forwards((3, 1)), refill, forwards((3, 3))))
     state = gather_start(1, after, x2)
-    near(6)
     far(6)
 
-    forwards((4, 1), (4, 2))()
+    forwards((4, 1), (4, 2), (5, 1))()
     relayed = gather_relay(state)
-    forwards((4, 3))()
+    forwards((4, 3), (6, 1))()
     gather_pass(state, relayed)
-    forwards((5, 1), (5, 2))()
+    forwards((5, 2))()
     gather_end(relayed)
-    forwards((6, 1))()
     with scope("norm2"):
         norm(x2, gain2, nb)
     forwards((6, 2))()
@@ -547,15 +564,10 @@
         arrive(4)
     last = (((1,), (1,)), ((), ()))
 
-    def ffn(i, carry):
-        at = span(i, LANES)
-        gate_val = lax.dot_general(nb[...], wgate[at, :], last, preferred_element_type=jnp.float32)
-        up_val = lax.dot_general(nb[...], wup[at, :], last, preferred_element_type=jnp.float32)
-        hid[:, at] = (jax.nn.silu(gate_val) * up_val).astype(jnp.bfloat16)
-        return carry
-
     with scope("ffn"):
-        lax.fori_loop(0, wgate.shape[0] // LANES, ffn, 0)
+        gate_val = lax.dot_general(nb[...], wgate[...], last, preferred_element_type=jnp.float32)
+        up_val = lax.dot_general(nb[...], wup[...], last, preferred_element_type=jnp.float32)
+        hid[...] = (jax.nn.silu(gate_val) * up_val).astype(jnp.bfloat16)
     forwards((5, 3), (6, 3))()
     with scope("arrive5"):
         arrive(5)

time: 88 us -> 86.2 us (0.980)
  Pallas kernels: 87.2 us -> 85 us
    pallas_call x1, Pallas kernels: 87.2 us -> 85 us  [on_device_paired(): pl.pallas_call(kernel, out_shape=jax.ShapeDtypeStruct((rows, feats), bf),...]
where the time goes in v3:
time: 86.2 us; the launch traced here: 85.6 us
  Pallas kernels  85 us (99%)
    pallas_call x1, Pallas kernels, on_device_paired(): pl.pallas_call(kernel, out_shape=jax.ShapeDtypeStruct((rows, feats), bf),...  85 us

profile of v3, /device:TPU:0, one launch (start us, length us, event | category | flops | bytes accessed | tf_op | source)
XLA Modules:
  0.0 85.6 jit_solution(7162509017327117749)
XLA Ops:
  0.0 85.0 %shard_map.127 = bf16[160,512]{1,0:T(8,128)(2,1)S(1)} custom-call(bf16[160,512]{1,0:T(8,128)(2,1)} %h_tok.1, f32[1,2048]{1,0:T(1,128)} %bitcast.7, bf16[256,256]{1,0:T(8,128)(2,1)} %h_x.1, bf16[256,256]{1,0:T(8,128)(2,1)} %h_g.1, f32[4,256]{1,0:T(4,128)} %h_taps.1, bf16[2,128,128]{2,1,0:T(8,128)(2,1)} %h_gxb.1, bf16[2,128,128]{2,1,0:T(8,128)(2,1)} %h_gab.1, ...), custom_call_target="tpu_custom_call" | custom-call | tf_op jit(solution)/shard_map/pallas_call | solution.py:616
  85.0 0.7 copy.15

commit v4 on v3

--- a/solution.py
+++ b/solution.py
@@ -246,20 +246,28 @@
             for group in names:
                 z_sends[group, 3].start()
 
-    def y_own(*names):
-        for group in names:
-            y_copies[group, 0] = send(
-                piece(group, h), place(group, f), send_y.at[group, 0], recv_y.at[group, 0], (fy, t)
-            )
+    for group in groups:
+        y_copies[group, 0] = describe(
+            piece(group, h), place(group, f), send_y.at[group, 0], recv_y.at[group, 0], (fy, t)
+        )
+        started.append(y_copies[group, 0])
+
+    def y_own(*names, role=None):
+        def go():
+            for group in names:
+                y_copies[group, 0].start()
+
+        go() if role is None else pl.when(role)(go)
 
     def pick(when_inner, when_outer):
         return jnp.where(inner, when_inner, when_outer)
 
     early = (pick(1, 3), pick(2, 1), pick(3, 2)), (pick(fz[1], fz[3]), pick(fz[2], fz[1]), pick(fz[3], fz[2]))
+    middle = (1, 3, 2), (fz[1], fz[3], fz[2])
     late = (1, pick(2, 3), pick(3, 2)), (fz[1], pick(fz[2], fz[3]), pick(fz[3], fz[2]))
 
     def forward(group, d):
-        arrival, arrival_fz = early if group < 5 else late
+        arrival, arrival_fz = early if group < 3 else middle if group < 5 else late
         block = place(group, arrival_fz[d - 1])
         describe(
             block, block, send_z.at[group, 0], recv_z.at[group, arrival[d - 1] - 1], (fz[1], t)
@@ -481,13 +489,16 @@
             z_sends[group, 3].start()
 
     y_own(2, 3)
+    y_own(5, role=outer)
     if fill:
         for w in (wgate, wup):
             w[pl.ds(half_ff, fill), :] = jnp.zeros((fill, model), jnp.bfloat16)
         for p in range(PARTS):
             wdn[p, pl.ds(half_ff, fill), :] = jnp.zeros((fill, wdn.shape[2]), jnp.bfloat16)
     relayed = gather_relay(state)
-    forwards((0, 1), (0, 2), (0, 3), (1, 1), (1, 2), (1, 3))()
+    forwards((0, 1), (0, 2), (0, 3), (1, 1), (1, 2))()
+    y_own(6, role=outer)
+    forwards((1, 3))()
     gather_pass(state, relayed)
     forwards((2, 1))()
     gather_end(relayed)
@@ -534,7 +545,8 @@
         decay = decay * shifted(decay, by, 1.0)
         by *= 2
     mix[...] = (run * jax.nn.gelu(branch_gate)).astype(jnp.bfloat16)
-    y_own(*groups[5:])
+    y_own(5, 6, role=inner)
+    forwards((3, 1))()
     with scope("arrive2"):
         arrive(2)
 
@@ -544,13 +556,13 @@
             near(5, 6)
 
         far(5)
-        forwards((3, 2))()
-
-    scatter(0, mix, wout, s1, s1r, k1, x1r, zs1, z1r, tok, after, (forwards((3, 1)), refill, forwards((3, 3))))
+        forwards((4, 1))()
+
+    scatter(0, mix, wout, s1, s1r, k1, x1r, zs1, z1r, tok, after, (forwards((3, 2)), refill, forwards((3, 3))))
     state = gather_start(1, after, x2)
     far(6)
 
-    forwards((4, 1), (4, 2), (5, 1))()
+    forwards((4, 2), (5, 1))()
     relayed = gather_relay(state)
     forwards((4, 3), (6, 1))()
     gather_pass(state, relayed)

time: 86.2 us -> 84 us (0.974)
  Pallas kernels: 85 us -> 83.2 us
    pallas_call x1, Pallas kernels: 85 us -> 83.2 us  [on_device_paired(): pl.pallas_call(kernel, out_shape=jax.ShapeDtypeStruct((rows, feats), bf),...]
where the time goes in v4:
time: 84 us; the launch traced here: 83.8 us
  Pallas kernels  83.2 us (99%)
    pallas_call x1, Pallas kernels, on_device_paired(): pl.pallas_call(kernel, out_shape=jax.ShapeDtypeStruct((rows, feats), bf),...  83.2 us

profile of v4, /device:TPU:0, one launch (start us, length us, event | category | flops | bytes accessed | tf_op | source)
XLA Modules:
  0.0 83.8 jit_solution(8831185879560645759)
XLA Ops:
  0.0 83.2 %shard_map.127 = bf16[160,512]{1,0:T(8,128)(2,1)S(1)} custom-call(bf16[160,512]{1,0:T(8,128)(2,1)} %h_tok.1, f32[1,2048]{1,0:T(1,128)} %bitcast.7, bf16[256,256]{1,0:T(8,128)(2,1)} %h_x.1, bf16[256,256]{1,0:T(8,128)(2,1)} %h_g.1, f32[4,256]{1,0:T(4,128)} %h_taps.1, bf16[2,128,128]{2,1,0:T(8,128)(2,1)} %h_gxb.1, bf16[2,128,128]{2,1,0:T(8,128)(2,1)} %h_gab.1, ...), custom_call_target="tpu_custom_call" | custom-call | tf_op jit(solution)/shard_map/pallas_call | solution.py:628
  83.2 0.7 copy.15

commit v5 on v4

--- a/solution.py
+++ b/solution.py
@@ -127,9 +127,10 @@
     h_tok, h_gain1, h_x, h_g, h_taps, h_gxb, h_gab, h_forget, h_out, h_gain2, h_gate, h_up, h_dn,
     result,
     tok, gain1, w_x, w_g, taps, gxb, gab, forget, w_out, gain2, w_gate, w_up, w_dn, load_sem,
-    x1, nb, win, wout, wgate, wup, wdn, s1, s1r, k1, x1r, zs1, z1r, after, mix, x2, hid,
-    s2, s2r, k2, x2r, zs2, z2r,
+    x1, nb, win, wout, wgate, wup, wdn, hidp, s1, s1r, k1, x1r, zs1, z1r, after, mix, x2, hid,
+    k2, x2r, zs2, z2r,
     send_z, recv_z, send_y, recv_y, own_sem, ag_send, ag_recv, rs_send, rs_recv, fin_send, fin_recv,
+    cross_recv, core_send, core_recv,
 ):
     f, t = lax.axis_index("fs"), lax.axis_index("tp")
     z, y = f // 2, f % 2
@@ -156,7 +157,7 @@
         load.start()
 
     barrier = pltpu.get_barrier_semaphore()
-    peers = [(fz[1], t), (fz[3], t), (fy, t), (f, t_core), (f, t_x)]
+    peers = [(fz[1], t), (fz[3], t), (fy, t), (fy, t_core), (f, t_core), (f, t_x)]
 
     def greet(peer):
         pl.semaphore_signal(barrier, inc=1, device_id=peer, device_id_type=pl.DeviceIdType.MESH)
@@ -193,7 +194,9 @@
     part_cols = cols // PARTS
     half_ff = w_dn.shape[0] // 2
     fill = wgate.shape[0] - half_ff
-    last_group = 4 + PARTS
+    last_group = 5 + PARTS
+    quarter = half_ff // 2
+    core = t % 2
 
     def piece(group, half, stored=False):
         if group < 2:
@@ -202,7 +205,10 @@
             return (h_out if stored else w_out).at[span(half, LANES), :]
         if group < 5:
             return ((h_gate, h_up) if stored else (w_gate, w_up))[group - 3].at[span(half, half_ff), :]
-        return (h_dn if stored else w_dn).at[span(half, half_ff), pl.ds((group - 5) * part_cols, part_cols)]
+        down = h_dn if stored else w_dn
+        if group == 5:
+            return down.at[span(half, half_ff), pl.ds(0, part_cols)]
+        return down.at[span(2 * half + group - 6, quarter), pl.ds(part_cols, part_cols)]
 
     def place(group, source):
         if group < 2:
@@ -211,7 +217,9 @@
             return wout.at[:, span(source, cols)]
         if group < 5:
             return (wgate, wup)[group - 3].at[pl.ds(0, half_ff), span(source, cols)]
-        return wdn.at[group - 5, pl.ds(0, half_ff), span(source, part_cols)]
+        if group == 5:
+            return wdn.at[0, core, pl.ds(0, half_ff), span(source, part_cols)]
+        return wdn.at[1, core, pl.ds((group - 6) * quarter, quarter), span(source, part_cols)]
 
     groups = range(last_group + 1)
     own_copies = {}
@@ -233,7 +241,7 @@
     y_copies, relays = {}, {}
 
     after_relay = {
-        0: ((2, 2), (2, 3)), 2: ((3, 2), (3, 3)), 3: ((4, 2), (4, 3)), 4: ((5, 2), (6, 2), (5, 3)), 6: ((6, 3),),
+        0: ((2, 2), (2, 3)), 2: ((3, 2), (3, 3)), 3: ((4, 2), (4, 3)), 4: ((5, 2), (5, 3)), 5: ((6, 2), (7, 2)), 6: ((6, 3),), 7: ((7, 3),),
     }
 
     def near(*names):
@@ -246,10 +254,25 @@
             for group in names:
                 z_sends[group, 3].start()
 
+    core_copies = []
+
+    def send_y_piece(group, d, src, dst, source_z):
+        if group < 5:
+            return describe(src, dst, send_y.at[group, d], recv_y.at[group, d], (fy, t))
+        arrived = cross_recv.at[group - 5, core, source_z // 2]
+        return describe(src, dst, send_y.at[group, d], arrived, (fy, t - core + source_z % 2))
+
+    def pass_to_core(group, d, src, dst, source_z):
+        if group >= 5:
+            copy = describe(
+                src, dst, core_send.at[group - 5, d], core_recv.at[group - 5, source_z // 2], (f, t_core)
+            )
+            other = source_z % 2 != core
+            core_copies.append((other, copy))
+            pl.when(other)(copy.start)
+
     for group in groups:
-        y_copies[group, 0] = describe(
-            piece(group, h), place(group, f), send_y.at[group, 0], recv_y.at[group, 0], (fy, t)
-        )
+        y_copies[group, 0] = send_y_piece(group, 0, piece(group, h), place(group, f), z)
         started.append(y_copies[group, 0])
 
     def y_own(*names, role=None):
@@ -258,6 +281,10 @@
                 y_copies[group, 0].start()
 
         go() if role is None else pl.when(role)(go)
+
+    def core_own():
+        for group in groups[5:]:
+            pass_to_core(group, 0, piece(group, h), place(group, f), z)
 
     def pick(when_inner, when_outer):
         return jnp.where(inner, when_inner, when_outer)
@@ -272,7 +299,10 @@
         describe(
             block, block, send_z.at[group, 0], recv_z.at[group, arrival[d - 1] - 1], (fz[1], t)
         ).wait_recv()
-        y_copies[group, d] = send(block, block, send_y.at[group, d], recv_y.at[group, d], (fy, t))
+        y_copies[group, d] = send_y_piece(group, d, block, block, arrival_fz[d - 1] // 2)
+        y_copies[group, d].start()
+        started.append(y_copies[group, d])
+        pass_to_core(group, d, block, block, arrival_fz[d - 1] // 2)
         if d == 1:
             relays[group] = describe(block, block, send_z.at[group, 3], recv_z.at[group, 1], (fz[2], t))
 
@@ -284,8 +314,14 @@
 
     def arrive(group):
         own_copies[group].wait()
-        for d in range(4):
-            y_copies[group, d].wait_recv()
+        if group < 5:
+            for d in range(4):
+                y_copies[group, d].wait_recv()
+            return
+        block = place(group, f)
+        ready = [cross_recv.at[group - 5, i, j] for i in range(2) for j in range(2)]
+        for semaphore in ready + [core_recv.at[group - 5, j] for j in range(2)]:
+            describe(block, block, send_y.at[group, 0], semaphore, (fy, t)).wait_recv()
 
     mine, theirs = span(h, rows), span(1 - h, rows)
     cut = rows // 2
@@ -393,38 +429,28 @@
         out[...] = (base[...].astype(jnp.float32) + (part + r3[...].astype(jnp.float32))).astype(jnp.bfloat16)
 
     def finish(p, acts):
-        core_peer, x_peer, z_peer = (f, t_core), (f, t_x), (fz[1], t)
+        x_peer, z_peer = (f, t_x), (fz[1], t)
         wide = feats // PARTS
         low, high = pl.ds(0, wide // 2), pl.ds(wide // 2, wide // 2)
-        s, r1, keep, r2, s3, r3 = s2.at[p], s2r.at[p], k2.at[p], x2r.at[p], zs2.at[p], z2r.at[p]
-
-        def project(block):
+        keep, r2, s3, r3 = k2.at[p], x2r.at[p], zs2.at[p], z2r.at[p]
+
+        def project_pair(block):
             at = span(block, wide)
-            s[:, at] = jnp.dot(acts[...], wdn[p, :, at], preferred_element_type=jnp.float32).astype(jnp.bfloat16)
-            return s.at[:, at]
+            return jnp.dot(acts[...], wdn[p, core, :, at], preferred_element_type=jnp.float32) + jnp.dot(
+                hidp[...], wdn[p, 1 - core, :, at], preferred_element_type=jnp.float32
+            )
 
         def go(i, src, dst, peer):
             return send(src, dst, fin_send.at[p, i], fin_recv.at[p, i], peer)
 
-        def pair_sum(block, i):
-            return s[:, span(block, wide)].astype(jnp.float32) + r1[i].astype(jnp.float32)
-
-        a = go(0, project(t_xc), r1.at[0], core_peer)
-        b = go(1, project(t_core), r1.at[1], core_peer)
-        project(t_x)
-        project(t)
         waits = {}
 
         def cross():
-            with scope(f"fin_a{p}"):
-                a.wait_recv()
-            keep[0] = pair_sum(t_x, 0).astype(jnp.bfloat16)
+            keep[0] = project_pair(t_x).astype(jnp.bfloat16)
             waits["d"] = go(3, keep.at[0, theirs, high], r3.at[0, :, high], z_peer)
             waits["c"] = go(2, keep.at[0, theirs, low], r2.at[theirs, low], x_peer)
             waits["m"] = go(7, keep.at[0, mine, low], r2.at[mine, low], x_peer)
-            with scope(f"fin_b{p}"):
-                b.wait_recv()
-            keep[1] = pair_sum(t, 1).astype(jnp.bfloat16)
+            keep[1] = project_pair(t).astype(jnp.bfloat16)
             waits["e"] = go(4, keep.at[1, theirs, high], r3.at[1, :, high], z_peer)
 
         def turn():
@@ -490,14 +516,16 @@
 
     y_own(2, 3)
     y_own(5, role=outer)
+    core_own()
     if fill:
         for w in (wgate, wup):
             w[pl.ds(half_ff, fill), :] = jnp.zeros((fill, model), jnp.bfloat16)
         for p in range(PARTS):
-            wdn[p, pl.ds(half_ff, fill), :] = jnp.zeros((fill, wdn.shape[2]), jnp.bfloat16)
+            for i in range(2):
+                wdn[p, i, pl.ds(half_ff, fill), :] = jnp.zeros((fill, wdn.shape[3]), jnp.bfloat16)
     relayed = gather_relay(state)
     forwards((0, 1), (0, 2), (0, 3), (1, 1), (1, 2))()
-    y_own(6, role=outer)
+    y_own(6, 7, role=outer)
     forwards((1, 3))()
     gather_pass(state, relayed)
     forwards((2, 1))()
@@ -512,7 +540,7 @@
 
     @pl.when(inner)
     def _():
-        near(5, 6)
+        near(5, 6, 7)
 
 
     with scope("arrive01"):
@@ -545,7 +573,7 @@
         decay = decay * shifted(decay, by, 1.0)
         by *= 2
     mix[...] = (run * jax.nn.gelu(branch_gate)).astype(jnp.bfloat16)
-    y_own(5, 6, role=inner)
+    y_own(5, 6, 7, role=inner)
     forwards((3, 1))()
     with scope("arrive2"):
         arrive(2)
@@ -553,24 +581,24 @@
     def refill():
         @pl.when(outer)
         def _():
-            near(5, 6)
+            near(5, 6, 7)
 
         far(5)
         forwards((4, 1))()
 
     scatter(0, mix, wout, s1, s1r, k1, x1r, zs1, z1r, tok, after, (forwards((3, 2)), refill, forwards((3, 3))))
     state = gather_start(1, after, x2)
-    far(6)
+    far(6, 7)
 
     forwards((4, 2), (5, 1))()
     relayed = gather_relay(state)
-    forwards((4, 3), (6, 1))()
+    forwards((4, 3), (6, 1), (7, 1))()
     gather_pass(state, relayed)
     forwards((5, 2))()
     gather_end(relayed)
     with scope("norm2"):
         norm(x2, gain2, nb)
-    forwards((6, 2))()
+    forwards((5, 3))()
     with scope("arrive34"):
         arrive(3)
         arrive(4)
@@ -580,13 +608,16 @@
         gate_val = lax.dot_general(nb[...], wgate[...], last, preferred_element_type=jnp.float32)
         up_val = lax.dot_general(nb[...], wup[...], last, preferred_element_type=jnp.float32)
         hid[...] = (jax.nn.silu(gate_val) * up_val).astype(jnp.bfloat16)
-    forwards((5, 3), (6, 3))()
+    hid_copy = send(hid, hidp, core_send.at[3, 0], core_recv.at[3, 0], (f, t_core))
+    forwards((6, 2), (7, 2), (6, 3), (7, 3))()
     with scope("arrive5"):
+        hid_copy.wait_recv()
         arrive(5)
     first = finish(0, hid)
     first[0]()
     with scope("arrive6"):
         arrive(6)
+        arrive(7)
     second = finish(1, hid)
     second[0]()
     first[1]()
@@ -596,6 +627,8 @@
     with scope("drain"):
         for copy in started:
             copy.wait_send()
+        for other, copy in core_copies:
+            pl.when(other)(copy.wait_send)
 
         @pl.when(inner)
         def _():
@@ -639,7 +672,8 @@
             pltpu.VMEM((LANES, model), bf),
             pltpu.VMEM((wide, model), bf),
             pltpu.VMEM((wide, model), bf),
-            pltpu.VMEM((PARTS, wide, model // PARTS), bf),
+            pltpu.VMEM((PARTS, 2, wide, model // PARTS), bf),
+            pltpu.VMEM((both, wide), bf),
             *exchange,
             pltpu.VMEM((rows, feats), bf),
             pltpu.VMEM((rows, feats), bf),
@@ -647,14 +681,13 @@
             pltpu.VMEM((both, LANES), bf),
             pltpu.VMEM((both, model), bf),
             pltpu.VMEM((both, wide), bf),
-            pltpu.VMEM((PARTS, both, model // PARTS), bf),
-            pltpu.VMEM((PARTS, 2, both, share), bf),
             pltpu.VMEM((PARTS, 2, both, share), bf),
             pltpu.VMEM((PARTS, both, share), bf),
             pltpu.VMEM((PARTS, rows, share), bf),
             pltpu.VMEM((PARTS, 2, rows, share), bf),
-            dma((7, 4)), dma((7, 3)), dma((7, 4)), dma((7, 4)), dma((7,)),
+            dma((8, 4)), dma((8, 3)), dma((8, 4)), dma((8, 4)), dma((8,)),
             dma((2, 11)), dma((2, 11)), dma((1, 5)), dma((1, 5)), dma((PARTS, 8)), dma((PARTS, 8)),
+            dma((3, 2, 2)), dma((4, 4)), dma((4, 2)),
         ],
         compiler_params=pltpu.CompilerParams(
             collective_id=0, has_side_effects=True, vmem_limit_bytes=48 * 1024 * 1024

time: 84 us -> 83 us (0.988)
  Pallas kernels: 83.2 us -> 82.2 us
    pallas_call x1, Pallas kernels: 83.2 us -> 82.2 us  [on_device_paired(): pl.pallas_call(kernel, out_shape=jax.ShapeDtypeStruct((rows, feats), bf),...]
where the time goes in v5:
time: 83 us; the launch traced here: 82.9 us
  Pallas kernels  82.2 us (99%)
    pallas_call x1, Pallas kernels, on_device_paired(): pl.pallas_call(kernel, out_shape=jax.ShapeDtypeStruct((rows, feats), bf),...  82.2 us

profile of v5, /device:TPU:0, one launch (start us, length us, event | category | flops | bytes accessed | tf_op | source)
XLA Modules:
  0.0 82.9 jit_solution(9676815659949561109)
XLA Ops:
  0.0 82.2 %shard_map.127 = bf16[160,512]{1,0:T(8,128)(2,1)S(1)} custom-call(bf16[160,512]{1,0:T(8,128)(2,1)} %h_tok.1, f32[1,2048]{1,0:T(1,128)} %bitcast.7, bf16[256,256]{1,0:T(8,128)(2,1)} %h_x.1, bf16[256,256]{1,0:T(8,128)(2,1)} %h_g.1, f32[4,256]{1,0:T(4,128)} %h_taps.1, bf16[2,128,128]{2,1,0:T(8,128)(2,1)} %h_gxb.1, bf16[2,128,128]{2,1,0:T(8,128)(2,1)} %h_gab.1, ...), custom_call_target="tpu_custom_call" | custom-call | tf_op jit(solution)/shard_map/pallas_call | solution.py:661
  82.2 0.7 copy.15

commit v6 on v5

--- a/solution.py
+++ b/solution.py
@@ -434,11 +434,12 @@
         low, high = pl.ds(0, wide // 2), pl.ds(wide // 2, wide // 2)
         keep, r2, s3, r3 = k2.at[p], x2r.at[p], zs2.at[p], z2r.at[p]
 
-        def project_pair(block):
+        def project_pair(i, block, where):
             at = span(block, wide)
-            return jnp.dot(acts[...], wdn[p, core, :, at], preferred_element_type=jnp.float32) + jnp.dot(
-                hidp[...], wdn[p, 1 - core, :, at], preferred_element_type=jnp.float32
-            )
+            keep[i, where, :] = (
+                jnp.dot(acts[where, :], wdn[p, core, :, at], preferred_element_type=jnp.float32)
+                + jnp.dot(hidp[where, :], wdn[p, 1 - core, :, at], preferred_element_type=jnp.float32)
+            ).astype(jnp.bfloat16)
 
         def go(i, src, dst, peer):
             return send(src, dst, fin_send.at[p, i], fin_recv.at[p, i], peer)
@@ -446,12 +447,14 @@
         waits = {}
 
         def cross():
-            keep[0] = project_pair(t_x).astype(jnp.bfloat16)
+            project_pair(0, t_x, theirs)
             waits["d"] = go(3, keep.at[0, theirs, high], r3.at[0, :, high], z_peer)
             waits["c"] = go(2, keep.at[0, theirs, low], r2.at[theirs, low], x_peer)
+            project_pair(1, t, theirs)
+            waits["e"] = go(4, keep.at[1, theirs, high], r3.at[1, :, high], z_peer)
+            project_pair(0, t_x, mine)
             waits["m"] = go(7, keep.at[0, mine, low], r2.at[mine, low], x_peer)
-            keep[1] = project_pair(t).astype(jnp.bfloat16)
-            waits["e"] = go(4, keep.at[1, theirs, high], r3.at[1, :, high], z_peer)
+            project_pair(1, t, mine)
 
         def turn():
             with scope(f"fin_d{p}"):
@@ -590,9 +593,9 @@
     state = gather_start(1, after, x2)
     far(6, 7)
 
-    forwards((4, 2), (5, 1))()
+    forwards((4, 2), (5, 1), (6, 1), (7, 1))()
     relayed = gather_relay(state)
-    forwards((4, 3), (6, 1), (7, 1))()
+    forwards((4, 3))()
     gather_pass(state, relayed)
     forwards((5, 2))()
     gather_end(relayed)
@@ -613,6 +616,7 @@
     with scope("arrive5"):
         hid_copy.wait_recv()
         arrive(5)
+    sent = len(started)
     first = finish(0, hid)
     first[0]()
     with scope("arrive6"):
@@ -622,19 +626,22 @@
     second[0]()
     first[1]()
     second[1]()
+    for copy in started[:sent]:
+        copy.wait_send()
+    for other, copy in core_copies:
+        pl.when(other)(copy.wait_send)
+
+    @pl.when(inner)
+    def _():
+        for group in groups:
+            z_sends[group, 2].wait_send()
+            relays[group].wait_send()
+
     first[2]()
     second[2]()
     with scope("drain"):
-        for copy in started:
+        for copy in started[sent:]:
             copy.wait_send()
-        for other, copy in core_copies:
-            pl.when(other)(copy.wait_send)
-
-        @pl.when(inner)
-        def _():
-            for group in groups:
-                z_sends[group, 2].wait_send()
-                relays[group].wait_send()
 
 
 def on_device_paired(

time: 83 us -> 82.7 us (level)
  no operation moved by 1% of the time
where the time goes in v6:
time: 82.7 us; the launch traced here: 82.6 us
  Pallas kernels  81.9 us (99%)
    pallas_call x1, Pallas kernels, on_device_paired(): pl.pallas_call(kernel, out_shape=jax.ShapeDtypeStruct((rows, feats), bf),...  81.9 us

profile of v6, /device:TPU:0, one launch (start us, length us, event | category | flops | bytes accessed | tf_op | source)
XLA Modules:
  0.0 82.6 jit_solution(18343790152431304428)
XLA Ops:
  0.0 81.9 %shard_map.127 = bf16[160,512]{1,0:T(8,128)(2,1)S(1)} custom-call(bf16[160,512]{1,0:T(8,128)(2,1)} %h_tok.1, f32[1,2048]{1,0:T(1,128)} %bitcast.7, bf16[256,256]{1,0:T(8,128)(2,1)} %h_x.1, bf16[256,256]{1,0:T(8,128)(2,1)} %h_g.1, f32[4,256]{1,0:T(4,128)} %h_taps.1, bf16[2,128,128]{2,1,0:T(8,128)(2,1)} %h_gxb.1, bf16[2,128,128]{2,1,0:T(8,128)(2,1)} %h_gab.1, ...), custom_call_target="tpu_custom_call" | custom-call | tf_op jit(solution)/shard_map/pallas_call | solution.py:668
  81.9 0.7 copy.15

commit v7 on v6

--- a/solution.py
+++ b/solution.py
@@ -241,7 +241,7 @@
     y_copies, relays = {}, {}
 
     after_relay = {
-        0: ((2, 2), (2, 3)), 2: ((3, 2), (3, 3)), 3: ((4, 2), (4, 3)), 4: ((5, 2), (5, 3)), 5: ((6, 2), (7, 2)), 6: ((6, 3),), 7: ((7, 3),),
+        0: ((2, 2), (2, 3)), 2: ((3, 2), (3, 3)), 3: ((4, 2), (4, 3)), 4: ((5, 2), (5, 3)), 5: ((6, 2), (7, 2)), 7: ((6, 3), (7, 3)),
     }
 
     def near(*names):

time: 82.7 us -> 82.7 us (level)
  no operation moved by 1% of the time
where the time goes in v7:
time: 82.7 us; the launch traced here: 82.6 us
  Pallas kernels  81.9 us (99%)
    pallas_call x1, Pallas kernels, on_device_paired(): pl.pallas_call(kernel, out_shape=jax.ShapeDtypeStruct((rows, feats), bf),...  81.9 us

profile of v7, /device:TPU:0, one launch (start us, length us, event | category | flops | bytes accessed | tf_op | source)
XLA Modules:
  0.0 82.6 jit_solution(9610088188378890115)
XLA Ops:
  0.0 81.9 %shard_map.127 = bf16[160,512]{1,0:T(8,128)(2,1)S(1)} custom-call(bf16[160,512]{1,0:T(8,128)(2,1)} %h_tok.1, f32[1,2048]{1,0:T(1,128)} %bitcast.7, bf16[256,256]{1,0:T(8,128)(2,1)} %h_x.1, bf16[256,256]{1,0:T(8,128)(2,1)} %h_g.1, f32[4,256]{1,0:T(4,128)} %h_taps.1, bf16[2,128,128]{2,1,0:T(8,128)(2,1)} %h_gxb.1, bf16[2,128,128]{2,1,0:T(8,128)(2,1)} %h_gab.1, ...), custom_call_target="tpu_custom_call" | custom-call | tf_op jit(solution)/shard_map/pallas_call | solution.py:668
  81.9 0.7 copy.15

commit v8 on v7

--- a/solution.py
+++ b/solution.py
@@ -601,7 +601,7 @@
     gather_end(relayed)
     with scope("norm2"):
         norm(x2, gain2, nb)
-    forwards((5, 3))()
+    forwards((5, 3), (6, 2))()
     with scope("arrive34"):
         arrive(3)
         arrive(4)
@@ -612,7 +612,7 @@
         up_val = lax.dot_general(nb[...], wup[...], last, preferred_element_type=jnp.float32)
         hid[...] = (jax.nn.silu(gate_val) * up_val).astype(jnp.bfloat16)
     hid_copy = send(hid, hidp, core_send.at[3, 0], core_recv.at[3, 0], (f, t_core))
-    forwards((6, 2), (7, 2), (6, 3), (7, 3))()
+    forwards((7, 2), (6, 3), (7, 3))()
     with scope("arrive5"):
         hid_copy.wait_recv()
         arrive(5)

time: 82.7 us -> 82.7 us (level)
  no operation moved by 1% of the time
where the time goes in v8:
time: 82.7 us; the launch traced here: 82.6 us
  Pallas kernels  81.9 us (99%)
    pallas_call x1, Pallas kernels, on_device_paired(): pl.pallas_call(kernel, out_shape=jax.ShapeDtypeStruct((rows, feats), bf),...  81.9 us

profile of v8, /device:TPU:0, one launch (start us, length us, event | category | flops | bytes accessed | tf_op | source)
XLA Modules:
  0.0 82.6 jit_solution(13328047134726544498)
XLA Ops:
  0.0 81.9 %shard_map.127 = bf16[160,512]{1,0:T(8,128)(2,1)S(1)} custom-call(bf16[160,512]{1,0:T(8,128)(2,1)} %h_tok.1, f32[1,2048]{1,0:T(1,128)} %bitcast.7, bf16[256,256]{1,0:T(8,128)(2,1)} %h_x.1, bf16[256,256]{1,0:T(8,128)(2,1)} %h_g.1, f32[4,256]{1,0:T(4,128)} %h_taps.1, bf16[2,128,128]{2,1,0:T(8,128)(2,1)} %h_gxb.1, bf16[2,128,128]{2,1,0:T(8,128)(2,1)} %h_gab.1, ...), custom_call_target="tpu_custom_call" | custom-call | tf_op jit(solution)/shard_map/pallas_call | solution.py:668
  81.9 0.7 copy.15

commit v9 on v8

--- a/solution.py
+++ b/solution.py
@@ -448,8 +448,8 @@
 
         def cross():
             project_pair(0, t_x, theirs)
+            waits["c"] = go(2, keep.at[0, theirs, low], r2.at[theirs, low], x_peer)
             waits["d"] = go(3, keep.at[0, theirs, high], r3.at[0, :, high], z_peer)
-            waits["c"] = go(2, keep.at[0, theirs, low], r2.at[theirs, low], x_peer)
             project_pair(1, t, theirs)
             waits["e"] = go(4, keep.at[1, theirs, high], r3.at[1, :, high], z_peer)
             project_pair(0, t_x, mine)

time: 82.7 us -> 82.7 us (level)
  no operation moved by 1% of the time
where the time goes in v9:
time: 82.7 us; the launch traced here: 82.6 us
  Pallas kernels  81.9 us (99%)
    pallas_call x1, Pallas kernels, on_device_paired(): pl.pallas_call(kernel, out_shape=jax.ShapeDtypeStruct((rows, feats), bf),...  81.9 us

profile of v9, /device:TPU:0, one launch (start us, length us, event | category | flops | bytes accessed | tf_op | source)
XLA Modules:
  0.0 82.6 jit_solution(12178557292208671954)
XLA Ops:
  0.0 81.9 %shard_map.127 = bf16[160,512]{1,0:T(8,128)(2,1)S(1)} custom-call(bf16[160,512]{1,0:T(8,128)(2,1)} %h_tok.1, f32[1,2048]{1,0:T(1,128)} %bitcast.7, bf16[256,256]{1,0:T(8,128)(2,1)} %h_x.1, bf16[256,256]{1,0:T(8,128)(2,1)} %h_g.1, f32[4,256]{1,0:T(4,128)} %h_taps.1, bf16[2,128,128]{2,1,0:T(8,128)(2,1)} %h_gxb.1, bf16[2,128,128]{2,1,0:T(8,128)(2,1)} %h_gab.1, ...), custom_call_target="tpu_custom_call" | custom-call | tf_op jit(solution)/shard_map/pallas_call | solution.py:668
  81.9 0.7 copy.15
